TPU v7x, 32 devices: a whole 2x2x4 slice. The times are simulated.
32 devices in a mesh: sp: 8 (over z, x), tp: 4 (over y, core).
Axes of the slice: x: 2, y: 2, z: 4, core: 2. Of those that a mesh axis runs over, the one named last changes fastest.
Arguments:
- latents: bfloat16 [4096, 2048], P(('sp', 'tp')), may hold values from -6 to 6
- context: bfloat16 [512, 2048], P('sp'), may hold values from -6 to 6
- cond: float32 [2048], P('sp'), may hold values from -6 to 6
- ctx_cond: float32 [2048], P('sp'), may hold values from -6 to 6
- mod_weight: float32 [2048, 6144], P('sp', 'tp'), may hold values from -0.125 to 0.125
- query_weight: bfloat16 [2048, 2048], P(None, 'tp'), may hold values from -1 to 1, as said below
- key_matrix: bfloat16 [2048, 1024], P(None, 'tp'), may hold values from -1 to 1, as said below
- value_matrix: bfloat16 [2048, 1024], P(None, 'tp'), may hold values from -0.125 to 0.125
- out_weight: bfloat16 [2048, 2048], P('tp'), may hold values from -0.125 to 0.125
- query_gain: float32 [128], replicated, may hold values from 0.7 to 7
- key_gain: float32 [128], replicated, may hold values from 0.7 to 7
Outputs:
- updated: bfloat16 [4096, 2048], P(('sp', 'tp'))
Inputs may be any that keep to these rules, and one draw needn't show every extreme that they name: `query_weight`: entries of order 2048 to the power -1/2. `key_matrix`: entries of order 2048 to the power -1/2.
All inputs are finite; a program needn't handle non-finite values.
Results may differ from a plain program's by a relative error of at most 0.0085.
The roundings to bfloat16 on the way count: a program that leaves them out, or rounds other values in their place, can miss the bound.
Values may be sent and summed in bfloat16 or wider, within the bound.
A program may use at most 128 MiB of HBM per device.

v0:
```python
import math
import jax
import jax.numpy as jnp
from jax import lax
from jax.sharding import PartitionSpec as P

GRID_W = 64
NORM_EPS = 1e-06
ROPE_BASE = 10000.0


def normalize(latent_value_rows):
    return latent_value_rows * lax.rsqrt(
        jnp.mean(latent_value_rows * latent_value_rows, axis=-1, keepdims=True) + NORM_EPS
    )


def rotate(latent_value_rows, positions):
    quarter = latent_value_rows.shape[-1] // 2
    inv_freq = ROPE_BASE ** (-jnp.arange(quarter, dtype=jnp.float32) / quarter)
    angles = positions.astype(jnp.float32)[:, None] * inv_freq[None, :]
    cos_table = jnp.cos(angles)[:, None, :]
    sin_table = jnp.sin(angles)[:, None, :]
    first, second = (latent_value_rows[..., :quarter], latent_value_rows[..., quarter:])
    return jnp.concatenate(
        [first * cos_table - second * sin_table, second * cos_table + first * sin_table], axis=-1
    )


def axial(latent_value_rows, positions):
    half_dim = latent_value_rows.shape[-1] // 2
    return jnp.concatenate(
        [
            rotate(latent_value_rows[..., :half_dim], positions // GRID_W),
            rotate(latent_value_rows[..., half_dim:], positions % GRID_W),
        ],
        axis=-1,
    )


def modulate(latent_value_rows, mod_row):
    model_width = latent_value_rows.shape[-1]
    shift_vec = mod_row[:model_width]
    scale_vec = mod_row[model_width : 2 * model_width]
    return (
        normalize(latent_value_rows.astype(jnp.float32)) * (1.0 + scale_vec) + shift_vec
    ).astype(jnp.bfloat16)


def body(
    latents,
    context,
    cond,
    ctx_cond,
    mod_weight,
    query_weight,
    key_matrix,
    value_matrix,
    out_weight,
    query_gain,
    key_gain,
):
    model_width = latents.shape[1]
    head_dim = query_gain.shape[0]
    sp_count = lax.axis_size("sp")
    partials = jnp.dot(
        jax.nn.silu(jnp.stack([cond, ctx_cond])), mod_weight, precision=lax.Precision.HIGHEST
    )
    summed = lax.psum(partials, "sp")
    modulation = lax.all_gather(summed, "tp", axis=1, tiled=True)
    gate_vec = modulation[0, 2 * model_width :]
    normalised_rows = modulate(latents, modulation[0])
    prefix_normalised = modulate(context, modulation[1])
    query_cols = query_weight.shape[1]
    key_cols = key_matrix.shape[1]
    piece = lax.all_gather(normalised_rows, "tp", axis=0, tiled=True)
    projected = jnp.concatenate(
        [
            jnp.dot(piece, query_weight, preferred_element_type=jnp.float32),
            jnp.dot(piece, key_matrix, preferred_element_type=jnp.float32),
            jnp.dot(piece, value_matrix, preferred_element_type=jnp.float32),
        ],
        axis=1,
    )
    row_count = projected.shape[0]
    positions = lax.axis_index("sp") * row_count + jnp.arange(row_count, dtype=jnp.int32)
    query_heads = projected[:, :query_cols].reshape(row_count, -1, head_dim)
    query_heads = axial(normalize(query_heads) * query_gain, positions).astype(jnp.bfloat16)
    key_heads = projected[:, query_cols : query_cols + key_cols].reshape(row_count, -1, head_dim)
    key_heads = axial(normalize(key_heads) * key_gain, positions).astype(jnp.bfloat16)
    value_heads = (
        projected[:, query_cols + key_cols :].reshape(row_count, -1, head_dim).astype(jnp.bfloat16)
    )
    key_part = jnp.dot(prefix_normalised, key_matrix, preferred_element_type=jnp.float32).reshape(
        prefix_normalised.shape[0], -1, head_dim
    )
    value_part = jnp.dot(
        prefix_normalised, value_matrix, preferred_element_type=jnp.float32
    ).reshape(prefix_normalised.shape[0], -1, head_dim)
    local_keys = (normalize(key_part) * key_gain).astype(jnp.bfloat16)
    local_values = value_part.astype(jnp.bfloat16)
    prefix_keys, prefix_values = (
        lax.all_gather(local_keys, "sp", axis=0, tiled=True),
        lax.all_gather(local_values, "sp", axis=0, tiled=True),
    )
    kv_local = key_heads.shape[1]
    group_size = query_heads.shape[1] // kv_local
    grouped = query_heads.reshape(row_count, kv_local, group_size, head_dim).transpose(1, 2, 0, 3)
    grouped = grouped.reshape(kv_local, group_size * row_count, head_dim)
    inv_root = head_dim ** (-0.5)
    lift = math.log(sp_count * row_count / (2.0 * prefix_keys.shape[0]))
    ctx_scores = (
        jnp.einsum("hqd,khd->hqk", grouped, prefix_keys, preferred_element_type=jnp.float32)
        * inv_root
        + lift
    )
    top_init = jnp.max(ctx_scores, axis=-1)
    ctx_weights = jnp.exp(ctx_scores - top_init[..., None])
    initial = (
        top_init,
        jnp.sum(ctx_weights, axis=-1),
        jnp.einsum(
            "hqk,khd->hqd",
            ctx_weights.astype(jnp.bfloat16),
            prefix_values,
            preferred_element_type=jnp.float32,
        ),
    )

    def update(state_now, key_block, value_block):
        top_old, total_old, acc_old = state_now
        scores = (
            jnp.einsum("hqd,khd->hqk", grouped, key_block, preferred_element_type=jnp.float32)
            * inv_root
        )
        top_new = jnp.maximum(top_old, jnp.max(scores, axis=-1))
        factor = jnp.exp(top_old - top_new)
        weights_now = jnp.exp(scores - top_new[..., None])
        acc_new = acc_old * factor[..., None] + jnp.einsum(
            "hqk,khd->hqd",
            weights_now.astype(jnp.bfloat16),
            value_block,
            preferred_element_type=jnp.float32,
        )
        return (top_new, total_old * factor + jnp.sum(weights_now, axis=-1), acc_new)

    key_piece = lax.all_gather(key_heads, "sp", axis=0, tiled=True)
    value_piece = lax.all_gather(value_heads, "sp", axis=0, tiled=True)
    key_count = key_piece.shape[0]
    rows_per_block = math.gcd(key_count, 2048)
    block_count = key_count // rows_per_block
    key_blocks = key_piece.reshape(block_count, rows_per_block, kv_local, head_dim)
    value_blocks = value_piece.reshape(block_count, rows_per_block, kv_local, head_dim)

    def one_step(state_in, blocks_in):
        return (update(state_in, blocks_in[0], blocks_in[1]), None)

    state_out, _ = lax.scan(one_step, initial, (key_blocks, value_blocks))
    top_fin, total_fin, acc_fin = state_out
    attended = (acc_fin / total_fin[..., None]).astype(jnp.bfloat16)
    attended = (
        attended.reshape(kv_local, group_size, row_count, head_dim)
        .transpose(2, 0, 1, 3)
        .reshape(row_count, -1)
    )
    mixed_rows = lax.psum_scatter(
        jnp.dot(attended, out_weight, preferred_element_type=jnp.float32).astype(jnp.bfloat16),
        "tp",
        scatter_dimension=0,
        tiled=True,
    ).astype(jnp.float32)
    return (latents.astype(jnp.float32) + gate_vec * normalize(mixed_rows)).astype(jnp.bfloat16)


def solution(mesh):
    placed = (
        P(("sp", "tp"), None),
        P("sp", None),
        P("sp"),
        P("sp"),
        P("sp", "tp"),
        P(None, "tp"),
        P(None, "tp"),
        P(None, "tp"),
        P("tp", None),
        P(),
        P(),
    )
    return jax.shard_map(
        body, mesh=mesh, in_specs=placed, out_specs=P(("sp", "tp"), None), check_vma=False
    )
```

profile of v0, /device:TPU:0, one launch (start us, length us, event | category | flops | bytes accessed | tf_op | source)
XLA Modules:
  0.0 286.1 jit_solution(9915169423210026204)
XLA Ops:
  6.5 2.4 fusion.41
  9.0 38.8 %psum.7 = f32[2,1536]{1,0:T(2,128)S(1)} all-reduce(f32[2,1536]{1,0:T(2,128)S(1)} %fusion.41), channel_id=1, replica_groups=mesh['sp'=8,'tp'=4] {'sp'}, use_global_device_ids=true, to_apply=%region_0.1 | all-reduce | flops 3072 | bytes 24576 | tf_op jit(solution)/shard_map/psum | solution.py:69
  47.8 5.2 %all_gather.18 = f32[2,6144]{1,0:T(2,128)S(1)} all-gather(f32[2,1536]{1,0:T(2,128)S(1)} %psum.7), channel_id=1, replica_groups=mesh['sp'=8,'tp'=4] {'tp'}, dimensions={1}, use_global_device_ids=true | all-gather | bytes 61440 | tf_op jit(solution)/shard_map/all_gather | solution.py:70
  54.9 2.1 fusion.30
  59.6 17.4 %all-gather.4.cloned.1.call-done = bf16[512,2048]{1,0:T(8,128)(2,1)} async-done(((bf16[128,2048]{1,0:T(8,128)(2,1)}), bf16[512,2048]{1,0:T(8,128)(2,1)}) %all-gather.4.cloned.1.call-update) | async-done | bytes 2097168 | tf_op jit(solution)/shard_map/all_gather | solution.py:76
  77.0 4.0 %multiply_reduce_fusion.1 = (f32[512,2]{0,1:T(2,128)}, f32[512,256]{0,1:T(8,128)}) fusion(bf16[512,2048]{1,0:T(8,128)(2,1)} %all-gather.4.cloned.1.call-done, bf16[2048,256]{1,0:T(8,128)(2,1)} %param.19), kind=kOutput, calls=%fused_computation.57 | convolution fusion | flops 537132032 | bytes 3674112 | tf_op jit(solution)/shard_map/dot_general | solution.py:80
  87.3 3.3 %convolution_convert_fusion.1 = bf16[512,256]{0,1:T(8,128)(2,1)} fusion(bf16[512,2048]{1,0:T(8,128)(2,1)} %all-gather.4.cloned.1.call-done, bf16[2048,256]{1,0:T(8,128)(2,1)} %param.20), kind=kOutput, calls=%fused_computation.32 | convolution fusion | flops 537001984 | bytes 3407872 | tf_op jit(solution)/shard_map/dot_general | solution.py:81
  98.4 31.6 %all_gather.20 = bf16[512,2,128]{2,0,1:T(8,128)(2,1)S(1)} all-gather(bf16[64,2,128]{2,0,1:T(8,128)(2,1)S(1)} %fusion.37), channel_id=1, replica_groups=mesh['sp'=8,'tp'=4] {'sp'}, dimensions={0}, use_global_device_ids=true | all-gather | bytes 294912 | tf_op jit(solution)/shard_map/all_gather | solution.py:103
  129.9 33.5 %all_gather.21 = bf16[512,2,128]{2,0,1:T(8,128)(2,1)} all-gather(bf16[64,2,128]{2,0,1:T(8,128)(2,1)S(1)} %bitcast.103), channel_id=1, replica_groups=mesh['sp'=8,'tp'=4] {'sp'}, dimensions={0}, use_global_device_ids=true | all-gather | bytes 294912 | tf_op jit(solution)/shard_map/all_gather | solution.py:104
  163.5 3.6 %multiply_reduce_fusion = (f32[512,4]{0,1:T(4,128)S(1)}, f32[512,512]{0,1:T(8,128)S(1)}) fusion(bf16[512,2048]{1,0:T(8,128)(2,1)} %all-gather.4.cloned.1.call-done, bf16[2048,512]{1,0:T(8,128)(2,1)} %param.18), kind=kOutput, calls=%fused_computation.44 | convolution fusion | flops 1074264064 | bytes 5251072 | tf_op jit(solution)/shard_map/dot_general | solution.py:79
  169.6 1.9 copy.74
  171.5 1.9 copy.75
  173.5 1.9 pad_maximum_fusion
  179.0 10.1 %all-gather.8.cloned.1.call-done = bf16[4096,2,128]{2,0,1:T(8,128)(2,1)} async-done(((bf16[512,2,128]{2,0,1:T(8,128)(2,1)}), bf16[4096,2,128]{2,0,1:T(8,128)(2,1)}) %all-gather.8.cloned.1.call-update) | async-done | bytes 2097168 | tf_op jit(solution)/shard_map/all_gather | solution.py:148
  189.1 52.1 %while.14 = (s32[]{:T(128)}, f32[2,1024]{1,0:T(2,128)S(1)}, f32[2,1024]{1,0:T(2,128)S(1)}, f32[2,1024,128]{2,1,0:T(8,128)S(1)}, bf16[2,2048,2,128]{3,1,0,2:T(8,1...) while((s32[]{:T(128)}, f32[2,1024]{1,0:T(2,128)S(1)}, ...), condition=%wide.region_11.12_spmd, body=%wide.region_8.11_spmd.sunk | while | flops 2181566464 | bytes 55182420 | solution.py:158
  189.1 9.4 %bitcast_reduce_fusion.2 = (f32[2,1024]{1,0:T(2,128)S(1)}, f32[2,2048,1024]{2,1,0:T(8,128)}) fusion(bf16[2,1024,128]{2,1,0:T(8,128)(2,1)} %get-tuple-element.194, bf16[2,2048,2,128]{3,1,0,2:T(8,128)(2,1)} %get-tuple-element.193, s32[]{:T(128)} %get-tuple-element.181), kind=kOutput, calls=%fused_computation.1.clone.1 | convolution fusion | flops 1082128384 | bytes 18358784 | tf_op jit(solution)/shard_map/while/body/eval_jaxpr/hqd,khd->hqk/dot_general | solution.py:133
  198.5 8.5 %fusion.80 = f32[2,1024]{1,0:T(2,128)S(1)} fusion(f32[2,2048,1024]{2,1,0:T(8,128)} %get-tuple-element.170, f32[2,1024]{1,0:T(2,128)S(1)} %max.4), kind=kLoop, calls=%fused_computation.4.clone.1 | loop fusion | flops 12580864 | bytes 16793600 | tf_op jit(solution)/shard_map/while/body/eval_jaxpr/reduce_sum | solution.py:145
  207.0 8.1 %fusion.81 = f32[2,1024,128]{2,1,0:T(8,128)S(1)} fusion(f32[2,2048,1024]{2,1,0:T(8,128)} %get-tuple-element.170, f32[2,1024]{1,0:T(2,128)S(1)} %max.4, bf16[2,2048,2,128]{3,1,0,2:T(8,128)(2,1)} %get-tuple-element.195, s32[]{:T(128)} %get-tuple-element.181, f32[2,1024,128]{2,1,0:T(8,128)S(1)} %get-tuple-element.184, f32[2,1024]{1,0:T(2,128)S(1)} %get-tuple-element.172), kind=kOutput, calls=%fused_computation.6.clone.1 | convolution fusion | flops 1086849024 | bytes 19939840 | tf_op jit(solution)/shard_map/while/body/eval_jaxpr/hqk,khd->hqd/dot_general | solution.py:139
  215.1 9.4 %bitcast_reduce_fusion.2 = (f32[2,1024]{1,0:T(2,128)S(1)}, f32[2,2048,1024]{2,1,0:T(8,128)}) fusion(bf16[2,1024,128]{2,1,0:T(8,128)(2,1)} %get-tuple-element.194, bf16[2,2048,2,128]{3,1,0,2:T(8,128)(2,1)} %get-tuple-element.193, s32[]{:T(128)} %get-tuple-element.181), kind=kOutput, calls=%fused_computation.1.clone.1 | convolution fusion | flops 1082128384 | bytes 18358784 | tf_op jit(solution)/shard_map/while/body/eval_jaxpr/hqd,khd->hqk/dot_general | solution.py:133
  224.5 8.5 %fusion.80 = f32[2,1024]{1,0:T(2,128)S(1)} fusion(f32[2,2048,1024]{2,1,0:T(8,128)} %get-tuple-element.170, f32[2,1024]{1,0:T(2,128)S(1)} %max.4), kind=kLoop, calls=%fused_computation.4.clone.1 | loop fusion | flops 12580864 | bytes 16793600 | tf_op jit(solution)/shard_map/while/body/eval_jaxpr/reduce_sum | solution.py:145
  233.1 8.1 %fusion.81 = f32[2,1024,128]{2,1,0:T(8,128)S(1)} fusion(f32[2,2048,1024]{2,1,0:T(8,128)} %get-tuple-element.170, f32[2,1024]{1,0:T(2,128)S(1)} %max.4, bf16[2,2048,2,128]{3,1,0,2:T(8,128)(2,1)} %get-tuple-element.195, s32[]{:T(128)} %get-tuple-element.181, f32[2,1024,128]{2,1,0:T(8,128)S(1)} %get-tuple-element.184, f32[2,1024]{1,0:T(2,128)S(1)} %get-tuple-element.172), kind=kOutput, calls=%fused_computation.6.clone.1 | convolution fusion | flops 1086849024 | bytes 19939840 | tf_op jit(solution)/shard_map/while/body/eval_jaxpr/hqk,khd->hqd/dot_general | solution.py:139
  243.6 2.6 convolution_convert_fusion
  246.3 29.9 %reduce-scatter.2.cloned.1.call-done = bf16[128,2048]{1,0:T(8,128)(2,1)} async-done(((bf16[512,2048]{1,0:T(8,128)(2,1)}), bf16[128,2048]{1,0:T(8,128)(2,1)}) %reduce-scatter.2.cloned.1.call-update) | async-done | bytes 524304 | tf_op jit(solution)/shard_map/reduce_scatter | solution.py:166
  277.4 2.1 fusion.31
  (79 shorter events, 28.3 us)
Async XLA Ops:
  6.5 237.1 %copy-start = (bf16[512,2048]{1,0:T(8,128)(2,1)S(1)}, bf16[512,2048]{1,0:T(8,128)(2,1)}, u32[]{:S(2)}) copy-start(bf16[512,2048]{1,0:T(8,128)(2,1)} %param.21) | copy-start | bytes 6291460
  6.5 70.5 %all-gather.4.cloned.1.call-start = ((), (), s32[]{:S(2)}) async-start(), calls=%async_computation.1 | async-start | bytes 2621440 | tf_op jit(solution)/shard_map/all_gather | solution.py:76
  57.0 122.0 %all-gather.6.cloned.1.call-start = ((), (), s32[]{:S(2)}) async-start(), calls=%async_computation.2 | async-start | bytes 2359296 | tf_op jit(solution)/shard_map/all_gather | solution.py:147
  57.6 19.4 %copy-start.6 = (f32[512,32]{0,1:T(8,128)}, f32[512,32]{0,1:T(8,128)S(1)}, u32[]{:S(2)}) copy-start(f32[512,32]{0,1:T(8,128)S(1)} %get-tuple-element.112) | copy-start | bytes 196612
  57.6 19.4 %copy-start.8 = (f32[512,32]{0,1:T(8,128)}, f32[512,32]{0,1:T(8,128)S(1)}, u32[]{:S(2)}) copy-start(f32[512,32]{0,1:T(8,128)S(1)} %get-tuple-element.113) | copy-start | bytes 196612
  81.0 5.5 %copy-start.3 = (bf16[64,2048]{1,0:T(8,128)(2,1)S(1)}, bf16[64,2048]{1,0:T(8,128)(2,1)}, u32[]{:S(2)}) copy-start(bf16[64,2048]{1,0:T(8,128)(2,1)} %param.14) | copy-start | bytes 786436
  85.3 8.4 %copy-start.4 = (bf16[2048,256]{1,0:T(8,128)(2,1)S(1)}, bf16[2048,256]{1,0:T(8,128)(2,1)}, u32[]{:S(2)}) copy-start(bf16[2048,256]{1,0:T(8,128)(2,1)} %param.19) | copy-start | bytes 3145732
  86.5 102.6 %all-gather.8.cloned.1.call-start = ((), (), s32[]{:S(2)}) async-start(), calls=%async_computation.3 | async-start | bytes 2359296 | tf_op jit(solution)/shard_map/all_gather | solution.py:148
  92.4 183.8 %reduce-scatter.2.cloned.1.call-start = ((), (), s32[]{:S(2)}) async-start(), calls=%async_computation.4 | async-start | bytes 2621440 | tf_op jit(solution)/shard_map/reduce_scatter | solution.py:166
  93.1 0.6 copy-start.11
  163.4 3.6 %copy-start.12 = (f32[128]{0:T(128)S(1)}, f32[128]{0:T(128)}, u32[]{:S(2)}) copy-start(f32[128]{0:T(128)} %param.22) | copy-start | bytes 1540
  163.4 3.8 %copy-start.7 = (f32[512,32]{0,1:T(8,128)S(1)}, f32[512,32]{0,1:T(8,128)}, u32[]{:S(2)}) copy-start(f32[512,32]{0,1:T(8,128)} %copy-done.6) | copy-start | bytes 196612
  163.4 3.8 %copy-start.9 = (f32[512,32]{0,1:T(8,128)S(1)}, f32[512,32]{0,1:T(8,128)}, u32[]{:S(2)}) copy-start(f32[512,32]{0,1:T(8,128)} %copy-done.8) | copy-start | bytes 196612
  175.3 0.8 copy-start.1
  176.1 1.6 copy-start.5
  243.6 33.8 %copy-start.2 = (bf16[128,2048]{1,0:T(8,128)(2,1)S(1)}, bf16[128,2048]{1,0:T(8,128)(2,1)}, u32[]{:S(2)}) copy-start(bf16[128,2048]{1,0:T(8,128)(2,1)} %param.13) | copy-start | bytes 1572868
  243.6 33.8 %copy-start.10 = (f32[1,2048]{1,0:T(1,128)S(1)}, f32[1,2048]{1,0:T(1,128)}, u32[]{:S(2)}) copy-start(f32[1,2048]{1,0:T(1,128)} %get-tuple-element.103) | copy-start | bytes 24580
Sparse Core Ops, SparseCore 0:
  57.1 19.8 all-gather.3
  86.6 52.3 all-gather.5
  141.2 47.7 all-gather.7
  246.4 29.7 reduce-scatter.1
where the time goes:
time: 287 us; the launch traced here: 286 us
  blocking collectives  109 us (38%)
  waiting for transfers between devices  57.5 us (20%)
  matrix products  55.5 us (19%)
  other arithmetic  36.5 us (13%)
  local copies, waits for them, and re-layouts  13.9 us (5%)
  between operations  13.4 us (5%)
    psum x1, blocking collectives, body(): summed = lax.psum(partials, 'sp')  38.8 us
    all_gather x1, blocking collectives, body(): lax.all_gather(local_values, 'sp', axis=0, tiled=True)  33.5 us
    all_gather x1, blocking collectives, body(): lax.all_gather(local_keys, 'sp', axis=0, tiled=True)  31.6 us
    reduce_scatter x1, waiting for transfers between devices, body(): lax.psum_scatter(jnp.dot(attended, out_weight, preferred_element_type=jnp...  29.9 us
    dot_general x2, matrix products, update(): jnp.einsum('hqd,khd->hqk', grouped, key_block, preferred_element_type=jnp...  18.8 us
    all_gather x1, waiting for transfers between devices, body(): piece = lax.all_gather(normalised_rows, 'tp', axis=0, tiled=True)  17.4 us
    reduce_sum x2, other arithmetic, update(): jnp.sum(weights_now, axis=-1)  17 us
    dot_general x2, matrix products, update(): jnp.einsum('hqk,khd->hqd', weights_now.astype(jnp.bfloat16), value_block,...  16.2 us
  transfers between devices with their start and end apart: 4, of which 3 were waited for; matrix products, arithmetic and copies ran while one was open for 10% of the time, Pallas kernels for 0%

commit v1 on v0

--- a/solution.py
+++ b/solution.py
@@ -73,7 +73,12 @@
     prefix_normalised = modulate(context, modulation[1])
     query_cols = query_weight.shape[1]
     key_cols = key_matrix.shape[1]
-    piece = lax.all_gather(normalised_rows, "tp", axis=0, tiled=True)
+    ring = [normalised_rows]
+    for hop in range(3):
+        ring.append(lax.ppermute(ring[-1], "tp", [(dev, (dev + 1) % 4) for dev in range(4)]))
+    piece = jnp.roll(
+        jnp.concatenate(ring[::-1], axis=0), (lax.axis_index("tp") + 1) * ring[0].shape[0], axis=0
+    )
     projected = jnp.concatenate(
         [
             jnp.dot(piece, query_weight, preferred_element_type=jnp.float32),

time: 287 us -> 294 us (1.024)
  local copies, waits for them, and re-layouts: 13.9 us -> 21.3 us
    ppermute x0 -> x3, waiting for transfers between devices: none -> 20.3 us  [body(): lax.ppermute(ring[-1], 'tp', [(dev, (dev + 1) % 4) for dev in range(4)])]
    all_gather x1 -> x0, waiting for transfers between devices: 17.4 us -> none  [body(): piece = lax.all_gather(normalised_rows, 'tp', axis=0, tiled=True)]
    unnamed x26 -> x44, local copies, waits for them, and re-layouts: 1.42 us -> 6.42 us
  transfers between devices with their start and end apart: 4 -> 6, of which waited for: 3 -> 5; matrix products, arithmetic and copies ran while one was open for 10% -> 11% of each run, Pallas kernels for 0% -> 0%
where the time goes in v1:
time: 294 us; the launch traced here: 293 us
  blocking collectives  109 us (37%)
  waiting for transfers between devices  57.9 us (20%)
  matrix products  53.8 us (18%)
  other arithmetic  36.7 us (12%)
  local copies, waits for them, and re-layouts  21.3 us (7%)
  between operations  13.5 us (5%)
    psum x1, blocking collectives, body(): summed = lax.psum(partials, 'sp')  38.8 us
    all_gather x1, blocking collectives, body(): lax.all_gather(local_values, 'sp', axis=0, tiled=True)  33.4 us
    all_gather x1, blocking collectives, body(): lax.all_gather(local_keys, 'sp', axis=0, tiled=True)  31.6 us
    reduce_scatter x1, waiting for transfers between devices, body(): lax.psum_scatter(jnp.dot(attended, out_weight, preferred_element_type=jnp...  29.9 us
    ppermute x3, waiting for transfers between devices, body(): lax.ppermute(ring[-1], 'tp', [(dev, (dev + 1) % 4) for dev in range(4)])  20.3 us
    dot_general x2, matrix products, update(): jnp.einsum('hqd,khd->hqk', grouped, key_block, preferred_element_type=jnp...  18.9 us
    reduce_sum x2, other arithmetic, update(): jnp.sum(weights_now, axis=-1)  17 us
    dot_general x2, matrix products, update(): jnp.einsum('hqk,khd->hqd', weights_now.astype(jnp.bfloat16), value_block,...  16.2 us
  transfers between devices with their start and end apart: 6, of which 5 were waited for; matrix products, arithmetic and copies ran while one was open for 11% of the time, Pallas kernels for 0%

profile of v1, /device:TPU:0, one launch (start us, length us, event | category | flops | bytes accessed | tf_op | source)
XLA Modules:
  0.0 292.7 jit_solution(2807044179396929721)
XLA Ops:
  6.5 2.4 fusion.50
  9.0 38.8 %psum.7 = f32[2,1536]{1,0:T(2,128)S(1)} all-reduce(f32[2,1536]{1,0:T(2,128)S(1)} %fusion.50), channel_id=1, replica_groups=mesh['sp'=8,'tp'=4] {'sp'}, use_global_device_ids=true, to_apply=%region_0.1 | all-reduce | flops 3072 | bytes 24576 | tf_op jit(solution)/shard_map/psum | solution.py:69
  47.8 5.2 %all_gather.15 = f32[2,6144]{1,0:T(2,128)S(1)} all-gather(f32[2,1536]{1,0:T(2,128)S(1)} %psum.7), channel_id=1, replica_groups=mesh['sp'=8,'tp'=4] {'tp'}, dimensions={1}, use_global_device_ids=true | all-gather | bytes 61440 | tf_op jit(solution)/shard_map/all_gather | solution.py:70
  57.1 8.3 %collective-permute-done = bf16[128,2048]{1,0:T(8,128)(2,1)S(1)} collective-permute-done((bf16[128,2048]{1,0:T(8,128)(2,1)S(1)}, bf16[128,2048]{1,0:T(8,128)(2,1)S(1)}, u32[]{:S(2)}, u32[]{:S(2)}) %collective-permute-start) | collective-permute-done | bytes 524320 | tf_op jit(solution)/shard_map/ppermute | solution.py:78
  65.3 8.7 %collective-permute-done.1 = bf16[128,2048]{1,0:T(8,128)(2,1)} collective-permute-done((bf16[128,2048]{1,0:T(8,128)(2,1)S(1)}, bf16[128,2048]{1,0:T(8,128)(2,1)}, u32[]{:S(2)}, u32[]{:S(2)}) %collective-permute-start.1) | collective-permute-done | bytes 524320 | tf_op jit(solution)/shard_map/ppermute | solution.py:78
  79.6 3.3 %collective-permute-done.2 = bf16[128,2048]{1,0:T(8,128)(2,1)} collective-permute-done((bf16[128,2048]{1,0:T(8,128)(2,1)}, bf16[128,2048]{1,0:T(8,128)(2,1)}, u32[]{:S(2)}, u32[]{:S(2)}) %collective-permute-start.2) | collective-permute-done | bytes 524320 | tf_op jit(solution)/shard_map/ppermute | solution.py:78
  88.5 2.0 multiply_reduce_fusion.1
  96.2 3.3 %fusion.30 = bf16[512,256]{0,1:T(8,128)(2,1)} fusion(bf16[2048,256]{1,0:T(8,128)(2,1)} %param.20, bf16[1024,2048]{1,0:T(8,128)(2,1)} %copy-done.13, s32[]{:T(128)S(6)} %select_n.36), kind=kOutput, calls=%fused_computation.38 | convolution fusion | flops 537001984 | bytes 3407876 | tf_op jit(solution)/shard_map/dot_general | solution.py:86
  107.3 31.6 %all_gather.16 = bf16[512,2,128]{2,0,1:T(8,128)(2,1)S(1)} all-gather(bf16[64,2,128]{2,0,1:T(8,128)(2,1)S(1)} %fusion.46), channel_id=1, replica_groups=mesh['sp'=8,'tp'=4] {'sp'}, dimensions={0}, use_global_device_ids=true | all-gather | bytes 294912 | tf_op jit(solution)/shard_map/all_gather | solution.py:108
  138.8 33.4 %all_gather.17 = bf16[512,2,128]{2,0,1:T(8,128)(2,1)} all-gather(bf16[64,2,128]{2,0,1:T(8,128)(2,1)S(1)} %bitcast.106), channel_id=1, replica_groups=mesh['sp'=8,'tp'=4] {'sp'}, dimensions={0}, use_global_device_ids=true | all-gather | bytes 294912 | tf_op jit(solution)/shard_map/all_gather | solution.py:109
  172.2 3.8 %multiply_reduce_fusion = (f32[512,4]{0,1:T(4,128)S(1)}, f32[512,512]{0,1:T(8,128)S(1)}) fusion(bf16[2048,512]{1,0:T(8,128)(2,1)} %param.18, bf16[1024,2048]{1,0:T(8,128)(2,1)} %copy-done.13, s32[]{:T(128)S(6)} %select_n.36), kind=kOutput, calls=%fused_computation.50 | convolution fusion | flops 1074264064 | bytes 5251076 | tf_op jit(solution)/shard_map/dot_general | solution.py:84
  178.7 1.9 copy.74
  180.6 1.9 copy.75
  188.0 7.7 %all-gather.5.cloned.1.call-done = bf16[4096,2,128]{2,0,1:T(8,128)(2,1)} async-done(((bf16[512,2,128]{2,0,1:T(8,128)(2,1)}), bf16[4096,2,128]{2,0,1:T(8,128)(2,1)}) %all-gather.5.cloned.1.call-update) | async-done | bytes 2097168 | tf_op jit(solution)/shard_map/all_gather | solution.py:153
  195.7 52.2 %while.14 = (s32[]{:T(128)}, f32[2,1024]{1,0:T(2,128)S(1)}, f32[2,1024]{1,0:T(2,128)S(1)}, f32[2,1024,128]{2,1,0:T(8,128)S(1)}, bf16[2,2048,2,128]{3,1,0,2:T(8,1...) while((s32[]{:T(128)}, f32[2,1024]{1,0:T(2,128)S(1)}, ...), condition=%wide.region_11.12_spmd, body=%wide.region_8.11_spmd.sunk | while | flops 2181566464 | bytes 55182420 | solution.py:163
  195.7 9.4 %bitcast_reduce_fusion.2 = (f32[2,1024]{1,0:T(2,128)S(1)}, f32[2,2048,1024]{2,1,0:T(8,128)}) fusion(bf16[2,1024,128]{2,1,0:T(8,128)(2,1)} %get-tuple-element.194, bf16[2,2048,2,128]{3,1,0,2:T(8,128)(2,1)} %get-tuple-element.193, s32[]{:T(128)} %get-tuple-element.181), kind=kOutput, calls=%fused_computation.1.clone.1 | convolution fusion | flops 1082128384 | bytes 18358784 | tf_op jit(solution)/shard_map/while/body/eval_jaxpr/hqd,khd->hqk/dot_general | solution.py:138
  205.1 8.5 %fusion.89 = f32[2,1024]{1,0:T(2,128)S(1)} fusion(f32[2,2048,1024]{2,1,0:T(8,128)} %get-tuple-element.170, f32[2,1024]{1,0:T(2,128)S(1)} %max.4), kind=kLoop, calls=%fused_computation.4.clone.1 | loop fusion | flops 12580864 | bytes 16793600 | tf_op jit(solution)/shard_map/while/body/eval_jaxpr/reduce_sum | solution.py:150
  213.7 8.1 %fusion.90 = f32[2,1024,128]{2,1,0:T(8,128)S(1)} fusion(f32[2,2048,1024]{2,1,0:T(8,128)} %get-tuple-element.170, f32[2,1024]{1,0:T(2,128)S(1)} %max.4, bf16[2,2048,2,128]{3,1,0,2:T(8,128)(2,1)} %get-tuple-element.195, s32[]{:T(128)} %get-tuple-element.181, f32[2,1024,128]{2,1,0:T(8,128)S(1)} %get-tuple-element.184, f32[2,1024]{1,0:T(2,128)S(1)} %get-tuple-element.172), kind=kOutput, calls=%fused_computation.6.clone.1 | convolution fusion | flops 1086849024 | bytes 19939840 | tf_op jit(solution)/shard_map/while/body/eval_jaxpr/hqk,khd->hqd/dot_general | solution.py:144
  221.8 9.4 %bitcast_reduce_fusion.2 = (f32[2,1024]{1,0:T(2,128)S(1)}, f32[2,2048,1024]{2,1,0:T(8,128)}) fusion(bf16[2,1024,128]{2,1,0:T(8,128)(2,1)} %get-tuple-element.194, bf16[2,2048,2,128]{3,1,0,2:T(8,128)(2,1)} %get-tuple-element.193, s32[]{:T(128)} %get-tuple-element.181), kind=kOutput, calls=%fused_computation.1.clone.1 | convolution fusion | flops 1082128384 | bytes 18358784 | tf_op jit(solution)/shard_map/while/body/eval_jaxpr/hqd,khd->hqk/dot_general | solution.py:138
  231.2 8.5 %fusion.89 = f32[2,1024]{1,0:T(2,128)S(1)} fusion(f32[2,2048,1024]{2,1,0:T(8,128)} %get-tuple-element.170, f32[2,1024]{1,0:T(2,128)S(1)} %max.4), kind=kLoop, calls=%fused_computation.4.clone.1 | loop fusion | flops 12580864 | bytes 16793600 | tf_op jit(solution)/shard_map/while/body/eval_jaxpr/reduce_sum | solution.py:150
  239.8 8.1 %fusion.90 = f32[2,1024,128]{2,1,0:T(8,128)S(1)} fusion(f32[2,2048,1024]{2,1,0:T(8,128)} %get-tuple-element.170, f32[2,1024]{1,0:T(2,128)S(1)} %max.4, bf16[2,2048,2,128]{3,1,0,2:T(8,128)(2,1)} %get-tuple-element.195, s32[]{:T(128)} %get-tuple-element.181, f32[2,1024,128]{2,1,0:T(8,128)S(1)} %get-tuple-element.184, f32[2,1024]{1,0:T(2,128)S(1)} %get-tuple-element.172), kind=kOutput, calls=%fused_computation.6.clone.1 | convolution fusion | flops 1086849024 | bytes 19939840 | tf_op jit(solution)/shard_map/while/body/eval_jaxpr/hqk,khd->hqd/dot_general | solution.py:144
  250.3 2.6 convolution_convert_fusion
  253.0 29.9 %reduce-scatter.2.cloned.1.call-done = bf16[128,2048]{1,0:T(8,128)(2,1)} async-done(((bf16[512,2048]{1,0:T(8,128)(2,1)}), bf16[128,2048]{1,0:T(8,128)(2,1)}) %reduce-scatter.2.cloned.1.call-update) | async-done | bytes 524304 | tf_op jit(solution)/shard_map/reduce_scatter | solution.py:171
  284.1 2.1 fusion.40
  (102 shorter events, 40.2 us)
Async XLA Ops:
  6.5 243.8 %copy-start = (bf16[512,2048]{1,0:T(8,128)(2,1)S(1)}, bf16[512,2048]{1,0:T(8,128)(2,1)}, u32[]{:S(2)}) copy-start(bf16[512,2048]{1,0:T(8,128)(2,1)} %param.21) | copy-start | bytes 6291460
  6.5 78.6 %copy-start.2 = (bf16[128,2048]{1,0:T(8,128)(2,1)S(1)}, bf16[128,2048]{1,0:T(8,128)(2,1)}, u32[]{:S(2)}) copy-start(bf16[128,2048]{1,0:T(8,128)(2,1)} %param.13) | copy-start | bytes 1572868
  6.5 181.5 %all-gather.3.cloned.1.call-start = ((), (), s32[]{:S(2)}) async-start(), calls=%async_computation.1 | async-start | bytes 2359296 | tf_op jit(solution)/shard_map/all_gather | solution.py:152
  56.7 8.7 %collective-permute-start = (bf16[128,2048]{1,0:T(8,128)(2,1)S(1)}, bf16[128,2048]{1,0:T(8,128)(2,1)S(1)}, u32[]{:S(2)}, u32[]{:S(2)}) collective-permute-start(bf16[128,2048]{1,0:T(8,128)(2,1)S(1)} %fusion.39), channel_id=1, source_target_pairs={{0,1},{1,2},{2,3},{3,0},{4,5},{5,6},{6,7},{7,4},{8,9},{9,10},{10,1... | collective-permute-start | bytes 1572872 | tf_op jit(solution)/shard_map/ppermute | solution.py:78
  65.3 8.7 %collective-permute-start.1 = (bf16[128,2048]{1,0:T(8,128)(2,1)S(1)}, bf16[128,2048]{1,0:T(8,128)(2,1)}, u32[]{:S(2)}, u32[]{:S(2)}) collective-permute-start(bf16[128,2048]{1,0:T(8,128)(2,1)S(1)} %collective-permute-done), channel_id=1, source_target_pairs={{0,1},{1,2},{2,3},{3,0},{4,5},{5,6},{6,7},{7,4},{8,9},{9,10},{10,1... | collective-permute-start | bytes 1572872 | tf_op jit(solution)/shard_map/ppermute | solution.py:78
  74.0 8.9 %collective-permute-start.2 = (bf16[128,2048]{1,0:T(8,128)(2,1)}, bf16[128,2048]{1,0:T(8,128)(2,1)}, u32[]{:S(2)}, u32[]{:S(2)}) collective-permute-start(bf16[128,2048]{1,0:T(8,128)(2,1)} %collective-permute-done.1), channel_id=1, source_target_pairs={{0,1},{1,2},{2,3},{3,0},{4,5},{5,6},{6,7},{7,4},{8,9},{9,10},{10,1... | collective-permute-start | bytes 1572872 | tf_op jit(solution)/shard_map/ppermute | solution.py:78
  79.6 8.6 %copy-start.16 = (f32[128]{0:T(128)S(1)}, f32[128]{0:T(128)}, u32[]{:S(2)}) copy-start(f32[128]{0:T(128)} %copy-done.15) | copy-start | bytes 1540
  79.6 8.9 %copy-start.6 = (bf16[2048,256]{1,0:T(8,128)(2,1)S(1)}, bf16[2048,256]{1,0:T(8,128)(2,1)}, u32[]{:S(2)}) copy-start(bf16[2048,256]{1,0:T(8,128)(2,1)} %param.19) | copy-start | bytes 3145732
  88.3 4.5 %copy-start.5 = (f32[512,32]{1,0:T(8,128)S(1)}, f32[512,32]{1,0:T(8,128)}, u32[]{:S(2)}) copy-start(f32[512,32]{1,0:T(8,128)} %copy.82) | copy-start | bytes 196612
  88.5 2.1 copy-start.13
  90.6 4.9 %copy-start.4 = (bf16[64,2048]{1,0:T(8,128)(2,1)S(1)}, bf16[64,2048]{1,0:T(8,128)(2,1)}, u32[]{:S(2)}) copy-start(bf16[64,2048]{1,0:T(8,128)(2,1)} %param.14) | copy-start | bytes 786436
  94.3 8.4 %copy-start.7 = (bf16[2048,256]{1,0:T(8,128)(2,1)S(1)}, bf16[2048,256]{1,0:T(8,128)(2,1)}, u32[]{:S(2)}) copy-start(bf16[2048,256]{1,0:T(8,128)(2,1)} %param.19) | copy-start | bytes 3145732
  94.3 8.4 %copy-start.11 = (f32[1,2048]{1,0:T(1,128)S(1)}, f32[1,2048]{1,0:T(1,128)}, u32[]{:S(2)}) copy-start(f32[1,2048]{1,0:T(1,128)} %get-tuple-element.104) | copy-start | bytes 24580
  94.3 8.4 %copy-start.12 = (f32[1,2048]{1,0:T(1,128)S(1)}, f32[1,2048]{1,0:T(1,128)}, u32[]{:S(2)}) copy-start(f32[1,2048]{1,0:T(1,128)} %get-tuple-element.105) | copy-start | bytes 24580
  95.4 100.3 %all-gather.5.cloned.1.call-start = ((), (), s32[]{:S(2)}) async-start(), calls=%async_computation.2 | async-start | bytes 2359296 | tf_op jit(solution)/shard_map/all_gather | solution.py:153
  101.4 181.5 %reduce-scatter.2.cloned.1.call-start = ((), (), s32[]{:S(2)}) async-start(), calls=%async_computation.3 | async-start | bytes 2621440 | tf_op jit(solution)/shard_map/reduce_scatter | solution.py:171
  102.1 0.6 copy-start.17
  172.2 3.9 %copy-start.18 = (f32[128]{0:T(128)S(1)}, f32[128]{0:T(128)}, u32[]{:S(2)}) copy-start(f32[128]{0:T(128)} %param.22) | copy-start | bytes 1540
  172.2 4.1 %copy-start.9 = (f32[512,32]{0,1:T(8,128)S(1)}, f32[512,32]{0,1:T(8,128)}, u32[]{:S(2)}) copy-start(f32[512,32]{0,1:T(8,128)} %get-tuple-element.112) | copy-start | bytes 196612
  172.2 4.1 %copy-start.10 = (f32[512,32]{0,1:T(8,128)S(1)}, f32[512,32]{0,1:T(8,128)}, u32[]{:S(2)}) copy-start(f32[512,32]{0,1:T(8,128)} %get-tuple-element.113) | copy-start | bytes 196612
  184.4 0.8 copy-start.1
  185.2 1.6 copy-start.8
  250.3 33.8 %copy-start.3 = (bf16[128,2048]{1,0:T(8,128)(2,1)S(1)}, bf16[128,2048]{1,0:T(8,128)(2,1)}, u32[]{:S(2)}) copy-start(bf16[128,2048]{1,0:T(8,128)(2,1)} %param.13) | copy-start | bytes 1572868
  250.3 33.8 %copy-start.14 = (f32[1,2048]{1,0:T(1,128)S(1)}, f32[1,2048]{1,0:T(1,128)}, u32[]{:S(2)}) copy-start(f32[1,2048]{1,0:T(1,128)} %get-tuple-element.103) | copy-start | bytes 24580
  (1 other events, 0.5 us)
Sparse Core Ops, SparseCore 0:
  95.5 49.0 all-gather.2
  146.8 48.8 all-gather.4
  253.1 29.7 reduce-scatter.1
